TPU v7x, 32 devices: a whole 2x2x4 slice. The times are simulated.
32 devices in a mesh: sp: 4 (over x, core), dp: 8 (over z, y).
Axes of the slice: x: 2, y: 2, z: 4, core: 2. Of those that a mesh axis runs over, the one named last changes fastest.
Arguments:
- tokens: bfloat16 [8, 1536, 2048], P('dp', 'sp'), may hold values from -6 to 6
- w_value: bfloat16 [2048, 1024], P('dp'), may hold values from -0.125 to 0.125
- w_gate: bfloat16 [2048, 1024], P('dp'), may hold values from -0.125 to 0.125
- conv_taps: bfloat16 [31, 1024], replicated, may hold values from -1 to 1
- norm_gain: bfloat16 [1024], replicated, may hold values from 0.099609375 to 1.8984375
- w_out: bfloat16 [1024, 2048], P(None, 'dp'), may hold values from -0.1875 to 0.1875
Outputs:
- mixed: bfloat16 [8, 1536, 2048], P('dp', 'sp')
All inputs are finite; a program needn't handle non-finite values.
Results may differ from a plain program's by a relative error of at most 0.013.
Values may be sent and summed in bfloat16 or wider, within the bound.
No kernel may reach another device: no remote copies, remote signals or barrier semaphores. Data moves between devices by JAX's collectives and lax.ppermute only.
A program may use at most 64 MiB of HBM per device.

v0:
```python
import jax
import jax.numpy as jnp
from jax import lax
from jax.sharding import PartitionSpec as P

EPSILON = 1e-06


def passed_along(x, axis, by):
    length = lax.axis_size(axis)
    pairs = [(i, i + by) for i in range(length) if 0 <= i + by < length]
    return lax.ppermute(x, axis, pairs)


def depthwise_conv(signal, local_taps, left_pad):
    kernel_form = jnp.transpose(local_taps)[:, None, :]
    result = lax.conv_general_dilated(
        signal[None],
        kernel_form,
        (1,),
        [(left_pad, 0)],
        dimension_numbers=("NCH", "OIH", "NCH"),
        feature_group_count=signal.shape[0],
        preferred_element_type=jnp.float32,
    )
    return result[0].astype(jnp.bfloat16)


def body(tokens, w_value, w_gate, conv_taps, norm_gain, w_out):
    seq_rows = tokens[0]
    tok_count = seq_rows.shape[0]
    kernel_len = conv_taps.shape[0]
    value_sum = jnp.einsum(
        "dc,td->ct",
        lax.all_gather(w_value, "dp", axis=0, tiled=True),
        seq_rows,
        preferred_element_type=jnp.float32,
    )
    gate_sum = jnp.einsum(
        "dc,td->ct",
        lax.all_gather(w_gate, "dp", axis=0, tiled=True),
        seq_rows,
        preferred_element_type=jnp.float32,
    )
    gated = (value_sum * jax.nn.sigmoid(gate_sum)).astype(jnp.bfloat16)
    last_rows = gated[:, tok_count - (kernel_len - 1) :]
    earlier = passed_along(last_rows, "sp", 1)
    extended = jnp.concatenate([earlier, gated], axis=1)
    conv_out = depthwise_conv(extended, conv_taps, 0)
    wide = conv_out.astype(jnp.float32)
    chan_mean = jnp.mean(wide, 0, keepdims=True)
    centred = wide - chan_mean
    chan_var = jnp.mean(centred * centred, 0, keepdims=True)
    normed = centred * lax.rsqrt(chan_var + EPSILON) * norm_gain.astype(jnp.float32)[:, None]
    activated = (normed * jax.nn.sigmoid(normed)).astype(jnp.bfloat16)
    projected = jnp.einsum(
        "ct,cd->td",
        activated,
        lax.all_gather(w_out, "dp", axis=1, tiled=True),
        preferred_element_type=jnp.float32,
    ).astype(jnp.bfloat16)
    return projected[None]


def solution(mesh):
    placed = (P("dp", "sp", None), P("dp", None), P("dp", None), P(), P(), P(None, "dp"))
    return jax.shard_map(
        body, mesh=mesh, in_specs=placed, out_specs=P("dp", "sp", None), check_vma=False
    )
```

profile of v0, /device:TPU:0, one launch (start us, length us, event | category | flops | bytes accessed | tf_op | source)
XLA Modules:
  0.0 246.4 jit_solution(6799378059922831921)
XLA Ops:
  6.5 0.7 all-gather.6.cloned.1.call-update
  7.3 0.0 all-gather.4.cloned.1.call-start
  7.3 0.7 all-gather.4.cloned.1.call-update
  8.0 0.0 all-gather.8.cloned.1.call-start
  8.1 0.7 all-gather.8.cloned.1.call-update
  8.7 76.3 %all-gather.6.cloned.1.call-done = bf16[2048,1024]{1,0:T(8,128)(2,1)} async-done(((bf16[256,1024]{1,0:T(8,128)(2,1)}), bf16[2048,1024]{1,0:T(8,128)(2,1)}) %all-gather.6.cloned.1.call-update) | async-done | bytes 4194320 | tf_op jit(solution)/shard_map/all_gather | solution.py:41
  85.0 4.0 %fusion.4 = f32[1024,384]{0,1:T(8,128)S(1)} fusion(bf16[2048,1024]{1,0:T(8,128)(2,1)} %all-gather.6.cloned.1.call-done, bf16[1,384,2048]{2,1,0:T(8,128)(2,1)S(1)} %copy-done), kind=kOutput, calls=%fused_computation.8 | convolution fusion | flops 1610612736 | bytes 7340032 | tf_op jit(solution)/shard_map/dc,td->ct/dot_general | solution.py:39
  89.0 69.5 %all-gather.4.cloned.1.call-done = bf16[2048,1024]{1,0:T(8,128)(2,1)} async-done(((bf16[256,1024]{1,0:T(8,128)(2,1)}), bf16[2048,1024]{1,0:T(8,128)(2,1)}) %all-gather.4.cloned.1.call-update) | async-done | bytes 4194320 | tf_op jit(solution)/shard_map/all_gather | solution.py:35
  158.5 4.1 %multiply_convert_fusion.1 = bf16[1024,384]{0,1:T(8,128)(2,1)S(1)} fusion(f32[1024,384]{0,1:T(8,128)S(1)} %fusion.4, bf16[2048,1024]{1,0:T(8,128)(2,1)} %all-gather.4.cloned.1.call-done, bf16[1,384,2048]{2,1,0:T(8,128)(2,1)S(1)} %copy-done), kind=kOutput, calls=%fused_computation.12 | convolution fusion | flops 1612578816 | bytes 8126464 | tf_op jit(solution)/shard_map/dc,td->ct/dot_general | solution.py:33
  162.6 1.3 collective-permute-start
  163.9 0.9 collective-permute-done
  164.8 0.2 maximum_bitcast_fusion
  165.0 0.1 pad
  165.0 0.2 reshape.17
  165.2 0.5 copy.12
  165.7 0.1 slice.7
  165.8 0.2 copy-done.2
  166.0 3.8 %fusion.17 = f32[8,52,1024]{2,0,1:T(8,128)S(1)} fusion(bf16[1024,1,7,30]{0,2,3,1:T(8,128)(2,1)S(1)} %slice.7, bf16[1024,1,8,52]{0,2,3,1:T(8,128)(2,1)S(1)} %copy.12, pred[8,52]{0,1:T(8,128)(4,1)S(1)} %copy-done.3, bf16[1024,1,31]{0,2,1:T(8,128)(2,1)S(1)} %bitcast.35), kind=kOutput, calls=%fused_computation.20 | convolution fusion | flops 31719424 | bytes 3049888 | tf_op jit(solution)/shard_map/conv_general_dilated | solution.py:17
  169.8 2.2 copy.14
  172.1 1.6 reshape.21
  173.7 0.2 slice_reduce_fusion
  173.8 0.3 multiply_reduce_fusion
  174.1 60.3 %all-gather.8.cloned.1.call-done = bf16[1024,2048]{1,0:T(8,128)(2,1)} async-done(((bf16[1024,256]{1,0:T(8,128)(2,1)}), bf16[1024,2048]{1,0:T(8,128)(2,1)}) %all-gather.8.cloned.1.call-update) | async-done | bytes 4194320 | tf_op jit(solution)/shard_map/all_gather | solution.py:59
  234.5 5.5 %fusion.1 = bf16[1,384,2048]{2,1,0:T(8,128)(2,1)} fusion(bf16[1024,2048]{1,0:T(8,128)(2,1)} %all-gather.8.cloned.1.call-done, f32[1,416,1024]{2,1,0:T(8,128)S(1)} %reshape.21, f32[1024]{0:T(1024)S(1)} %convert_element_type.26, f32[384]{0:T(512)S(1)} %add_rsqrt_fusion, f32[384]{0:T(512)S(1)} %broadcast_multiply_fusion), kind=kOutput, calls=%fused_computation.3 | convolution fusion | flops 1614544896 | bytes 7348224 | tf_op jit(solution)/shard_map/ct,cd->td/dot_general | solution.py:56
  (12 shorter events, 0.1 us)
Async XLA Ops:
  6.5 78.5 %copy-start = (bf16[1,384,2048]{2,1,0:T(8,128)(2,1)S(1)}, bf16[1,384,2048]{2,1,0:T(8,128)(2,1)}, u32[]{:S(2)}) copy-start(bf16[1,384,2048]{2,1,0:T(8,128)(2,1)} %param.6) | copy-start | bytes 4718596
  6.5 78.5 %all-gather.6.cloned.1.call-start = ((), (), s32[]{:S(2)}) async-start(), calls=%async_computation.1 | async-start | bytes 4718592 | tf_op jit(solution)/shard_map/all_gather | solution.py:41
  7.3 151.2 %all-gather.4.cloned.1.call-start = ((), (), s32[]{:S(2)}) async-start(), calls=%async_computation | async-start | bytes 4718592 | tf_op jit(solution)/shard_map/all_gather | solution.py:35
  8.0 226.4 %all-gather.8.cloned.1.call-start = ((), (), s32[]{:S(2)}) async-start(), calls=%async_computation.2 | async-start | bytes 4718592 | tf_op jit(solution)/shard_map/all_gather | solution.py:59
  89.0 74.9 %copy-start.1 = (bf16[1024]{0:T(1024)(128)(2,1)S(1)}, bf16[1024]{0:T(1024)(128)(2,1)}, u32[]{:S(2)}) copy-start(bf16[1024]{0:T(1024)(128)(2,1)} %param.10) | copy-start | bytes 6148
  162.6 2.2 collective-permute-start
  165.2 0.8 copy-start.2
  165.2 0.8 copy-start.3
Sparse Core Ops, SparseCore 0:
  9.5 75.5 all-gather.5
  87.1 71.3 all-gather.3
  160.5 73.8 all-gather.7
where the time goes:
time: 247 us; the launch traced here: 246 us
  waiting for transfers between devices  209 us (85%)
  matrix products  17.3 us (7%)
  between operations  13.2 us (5%)
  local copies, waits for them, and re-layouts  4.87 us (2%)
    all_gather x1, waiting for transfers between devices, body(): lax.all_gather(w_gate, 'dp', axis=0, tiled=True)  76.3 us
    all_gather x1, waiting for transfers between devices, body(): lax.all_gather(w_value, 'dp', axis=0, tiled=True)  69.5 us
    all_gather x1, waiting for transfers between devices, body(): lax.all_gather(w_out, 'dp', axis=1, tiled=True)  60.3 us
    dot_general x1, matrix products, body(): jnp.einsum('ct,cd->td', activated, lax.all_gather(w_out, 'dp', axis=1, ti...  5.46 us
  transfers between devices with their start and end apart: 4, of which 4 were waited for; matrix products, arithmetic and copies ran while one was open for 7% of the time, Pallas kernels for 0%

commit v1 on v0

--- a/solution.py
+++ b/solution.py
@@ -4,6 +4,27 @@
 from jax.sharding import PartitionSpec as P
 
 EPSILON = 1e-06
+
+
+def get_meshes_on(local_x, lane_axis, array_axis, buf, which_dim):
+    mixed_arr = jax.lax.axis_size(lane_axis)
+    z2, reached, top = (mixed_arr, jax.lax.axis_index(lane_axis), local_x.shape[array_axis])
+    extra = carry_in = local_x
+    frame_out, built = ([], [])
+    for num in tuple(range(z2 // 2 + 1)):
+        frame_out.append(buf(extra, (reached - num) % z2 * top))
+        if 0 < num < z2 - z2 // 2:
+            built.append(buf(carry_in, (reached + num) % z2 * top))
+        table = []
+        for dd in tuple(range(z2)):
+            table.append((dd, (dd + 1) % z2))
+        extra = jax.lax.ppermute(extra, lane_axis, table)
+        slots = []
+        for dd in tuple(range(z2)):
+            slots.append((dd, (dd - 1) % z2))
+        carry_in = jax.lax.ppermute(carry_in, lane_axis, slots)
+    moved = jnp.concatenate([*frame_out[::-1], *built], axis=which_dim)
+    return jnp.roll(moved, (reached - z2 // 2) * frame_out[0].shape[which_dim], axis=which_dim)
 
 
 def passed_along(x, axis, by):
@@ -53,11 +74,14 @@
     chan_var = jnp.mean(centred * centred, 0, keepdims=True)
     normed = centred * lax.rsqrt(chan_var + EPSILON) * norm_gain.astype(jnp.float32)[:, None]
     activated = (normed * jax.nn.sigmoid(normed)).astype(jnp.bfloat16)
-    projected = jnp.einsum(
-        "ct,cd->td",
-        activated,
-        lax.all_gather(w_out, "dp", axis=1, tiled=True),
-        preferred_element_type=jnp.float32,
+    projected = get_meshes_on(
+        w_out,
+        "dp",
+        array_axis=1,
+        buf=lambda shard, start: jnp.einsum(
+            "ct,cd->td", activated, shard, preferred_element_type=jnp.float32
+        ),
+        which_dim=1,
     ).astype(jnp.bfloat16)
     return projected[None]
 

time: 247 us -> 238 us (0.964)
  waiting for transfers between devices: 209 us -> 175 us
  starting transfers between devices: 1.37 us -> 18.6 us
  matrix products: 17.3 us -> 21.9 us
    ppermute x0 -> x7, waiting for transfers between devices: none -> 63.4 us  [the longest x4 63.4 us: get_meshes_on(): extra = jax.lax.ppermute(extra, lane_axis, table)]
    all_gather x1 -> x0, waiting for transfers between devices: 60.3 us -> none  [body(): lax.all_gather(w_out, 'dp', axis=1, tiled=True)]
    all_gather x1, waiting for transfers between devices: 76.3 us -> 41.5 us  [body(): lax.all_gather(w_gate, 'dp', axis=0, tiled=True)]
    ppermute x0 -> x7, starting transfers between devices: none -> 17.2 us  [the longest x3 9.34 us: get_meshes_on(): carry_in = jax.lax.ppermute(carry_in, lane_axis, slots)]
    dot_general x1 -> x8, matrix products: 5.46 us -> 8.38 us  [body(): jnp.einsum('ct,cd->td', activated, shard, preferred_element_type=jnp.floa...]
  transfers between devices with their start and end apart: 4 -> 10, of which waited for: 4 -> 5; matrix products, arithmetic and copies ran while one was open for 7% -> 11% of each run, Pallas kernels for 0% -> 0%
where the time goes in v1:
time: 238 us; the launch traced here: 237 us
  waiting for transfers between devices  175 us (74%)
  matrix products  21.9 us (9%)
  starting transfers between devices  18.6 us (8%)
  between operations  13.8 us (6%)
  local copies, waits for them, and re-layouts  6.78 us (3%)
    all_gather x1, waiting for transfers between devices, body(): lax.all_gather(w_value, 'dp', axis=0, tiled=True)  68.5 us
    ppermute x4, waiting for transfers between devices, get_meshes_on(): extra = jax.lax.ppermute(extra, lane_axis, table)  63.4 us
    all_gather x1, waiting for transfers between devices, body(): lax.all_gather(w_gate, 'dp', axis=0, tiled=True)  41.5 us
    ppermute x3, starting transfers between devices, get_meshes_on(): carry_in = jax.lax.ppermute(carry_in, lane_axis, slots)  9.34 us
    dot_general x8, matrix products, body(): jnp.einsum('ct,cd->td', activated, shard, preferred_element_type=jnp.floa...  8.38 us
    ppermute x4, starting transfers between devices, get_meshes_on(): extra = jax.lax.ppermute(extra, lane_axis, table)  7.91 us
    dot_general x1, matrix products, body(): jnp.einsum('dc,td->ct', lax.all_gather(w_gate, 'dp', axis=0, tiled=True),...  5.12 us
  transfers between devices with their start and end apart: 10, of which 5 were waited for; matrix products, arithmetic and copies ran while one was open for 11% of the time, Pallas kernels for 0%

profile of v1, /device:TPU:0, one launch (start us, length us, event | category | flops | bytes accessed | tf_op | source)
XLA Modules:
  0.0 237.2 jit_solution(17859248095704365101)
XLA Ops:
  6.5 0.7 all-gather.5.cloned.1.call-update
  7.3 0.7 all-gather.3.cloned.1.call-update
  8.0 3.0 %collective-permute-start.1 = (bf16[1024,256]{1,0:T(8,128)(2,1)}, bf16[1024,256]{1,0:T(8,128)(2,1)S(1)}, u32[]{:S(2)}, u32[]{:S(2)}) collective-permute-start(bf16[1024,256]{1,0:T(8,128)(2,1)} %param.11), channel_id=1, source_target_pairs={{0,1},{1,2},{2,3},{3,4},{4,5},{5,6},{6,7},{7,0},{8,9},{9,10},{10,1... | collective-permute-start | bytes 1572872 | tf_op jit(solution)/shard_map/ppermute | solution.py:21
  11.1 3.1 %collective-permute-start.5 = (bf16[1024,256]{1,0:T(8,128)(2,1)}, bf16[1024,256]{1,0:T(8,128)(2,1)S(1)}, u32[]{:S(2)}, u32[]{:S(2)}) collective-permute-start(bf16[1024,256]{1,0:T(8,128)(2,1)} %param.11), channel_id=1, source_target_pairs={{0,7},{1,0},{2,1},{3,2},{4,3},{5,4},{6,5},{7,6},{8,15},{9,8},{10,9... | collective-permute-start | bytes 1572872 | tf_op jit(solution)/shard_map/ppermute | solution.py:25
  14.2 25.2 %collective-permute-done.1 = bf16[1024,256]{1,0:T(8,128)(2,1)S(1)} collective-permute-done((bf16[1024,256]{1,0:T(8,128)(2,1)}, bf16[1024,256]{1,0:T(8,128)(2,1)S(1)}, u32[]{:S(2)}, u32[]{:S(2)}) %collective-permute-start.1) | collective-permute-done | bytes 524320 | tf_op jit(solution)/shard_map/ppermute | solution.py:21
  39.4 2.4 %collective-permute-start.2 = (bf16[1024,256]{1,0:T(8,128)(2,1)S(1)}, bf16[1024,256]{1,0:T(8,128)(2,1)S(1)}, u32[]{:S(2)}, u32[]{:S(2)}) collective-permute-start(bf16[1024,256]{1,0:T(8,128)(2,1)S(1)} %collective-permute-done.1), channel_id=1, source_target_pairs={{0,1},{1,2},{2,3},{3,4},{4,5},{5,6},{6,7},{7,0},{8,9},{9,10},{10,1... | collective-permute-start | bytes 1572872 | tf_op jit(solution)/shard_map/ppermute | solution.py:21
  41.8 3.9 %collective-permute-start.6 = (bf16[1024,256]{1,0:T(8,128)(2,1)S(1)}, bf16[1024,256]{1,0:T(8,128)(2,1)}, u32[]{:S(2)}, u32[]{:S(2)}) collective-permute-start(bf16[1024,256]{1,0:T(8,128)(2,1)S(1)} %collective-permute-done.5), channel_id=1, source_target_pairs={{0,7},{1,0},{2,1},{3,2},{4,3},{5,4},{6,5},{7,6},{8,15},{9,8},{10,9... | collective-permute-start | bytes 1572872 | tf_op jit(solution)/shard_map/ppermute | solution.py:25
  45.7 25.1 %collective-permute-done.2 = bf16[1024,256]{1,0:T(8,128)(2,1)S(1)} collective-permute-done((bf16[1024,256]{1,0:T(8,128)(2,1)S(1)}, bf16[1024,256]{1,0:T(8,128)(2,1)S(1)}, u32[]{:S(2)}, u32[]{:S(2)}) %collective-permute-start.2) | collective-permute-done | bytes 524320 | tf_op jit(solution)/shard_map/ppermute | solution.py:21
  70.8 2.5 %collective-permute-start.3 = (bf16[1024,256]{1,0:T(8,128)(2,1)S(1)}, bf16[1024,256]{1,0:T(8,128)(2,1)}, u32[]{:S(2)}, u32[]{:S(2)}) collective-permute-start(bf16[1024,256]{1,0:T(8,128)(2,1)S(1)} %collective-permute-done.2), channel_id=1, source_target_pairs={{0,1},{1,2},{2,3},{3,4},{4,5},{5,6},{6,7},{7,0},{8,9},{9,10},{10,1... | collective-permute-start | bytes 1572872 | tf_op jit(solution)/shard_map/ppermute | solution.py:21
  73.3 41.5 %all-gather.5.cloned.1.call-done = bf16[2048,1024]{1,0:T(8,128)(2,1)} async-done(((bf16[256,1024]{1,0:T(8,128)(2,1)}), bf16[2048,1024]{1,0:T(8,128)(2,1)}) %all-gather.5.cloned.1.call-update) | async-done | bytes 4194320 | tf_op jit(solution)/shard_map/all_gather | solution.py:62
  114.8 5.1 %fusion.4 = f32[1024,384]{0,1:T(8,128)} fusion(bf16[2048,1024]{1,0:T(8,128)(2,1)} %all-gather.5.cloned.1.call-done, bf16[1,384,2048]{2,1,0:T(8,128)(2,1)S(1)} %copy-done), kind=kOutput, calls=%fused_computation.8 | convolution fusion | flops 1610612736 | bytes 7340032 | tf_op jit(solution)/shard_map/dc,td->ct/dot_general | solution.py:60
  119.9 68.5 %all-gather.3.cloned.1.call-done = bf16[2048,1024]{1,0:T(8,128)(2,1)} async-done(((bf16[256,1024]{1,0:T(8,128)(2,1)}), bf16[2048,1024]{1,0:T(8,128)(2,1)}) %all-gather.3.cloned.1.call-update) | async-done | bytes 4194320 | tf_op jit(solution)/shard_map/all_gather | solution.py:56
  188.5 4.5 %multiply_convert_fusion.1 = bf16[1024,384]{0,1:T(8,128)(2,1)S(1)} fusion(f32[1024,384]{0,1:T(8,128)} %fusion.4, bf16[2048,1024]{1,0:T(8,128)(2,1)} %all-gather.3.cloned.1.call-done, bf16[1,384,2048]{2,1,0:T(8,128)(2,1)S(1)} %copy-done), kind=kOutput, calls=%fused_computation.12 | convolution fusion | flops 1612578816 | bytes 8126464 | tf_op jit(solution)/shard_map/dc,td->ct/dot_general | solution.py:54
  193.1 1.3 collective-permute-start
  194.4 2.3 collective-permute-start.7
  197.9 3.9 %fusion.17 = f32[8,52,1024]{2,0,1:T(8,128)S(1)} fusion(bf16[1024,1,7,30]{0,2,3,1:T(8,128)(2,1)S(1)} %slice.7, bf16[1024,1,8,52]{0,2,3,1:T(8,128)(2,1)S(1)} %copy.13, pred[8,52]{0,1:T(8,128)(4,1)S(1)} %copy-done.10, bf16[1024,1,31]{0,2,1:T(8,128)(2,1)S(1)} %bitcast.49), kind=kOutput, calls=%fused_computation.20 | convolution fusion | flops 31719424 | bytes 3049888 | tf_op jit(solution)/shard_map/conv_general_dilated | solution.py:38
  201.8 2.2 copy.15
  204.0 1.6 reshape.21
  206.7 13.1 %collective-permute-done.4 = bf16[1024,256]{1,0:T(8,128)(2,1)} collective-permute-done((bf16[1024,256]{1,0:T(8,128)(2,1)}, bf16[1024,256]{1,0:T(8,128)(2,1)}, u32[]{:S(2)}, u32[]{:S(2)}) %collective-permute-start.4) | collective-permute-done | bytes 524320 | tf_op jit(solution)/shard_map/ppermute | solution.py:21
  219.7 1.5 constant_dynamic-update-slice_fusion.15
  221.3 1.6 constant_dynamic-update-slice_fusion.14
  225.1 1.6 constant_dynamic-update-slice_fusion.9
  226.7 1.6 constant_dynamic-update-slice_fusion.8
  228.7 1.6 copy.16
  (55 shorter events, 4.8 us)
Async XLA Ops:
  6.5 108.3 %copy-start = (bf16[1,384,2048]{2,1,0:T(8,128)(2,1)S(1)}, bf16[1,384,2048]{2,1,0:T(8,128)(2,1)}, u32[]{:S(2)}) copy-start(bf16[1,384,2048]{2,1,0:T(8,128)(2,1)} %param.6) | copy-start | bytes 4718596
  6.5 108.3 %all-gather.5.cloned.1.call-start = ((), (), s32[]{:S(2)}) async-start(), calls=%async_computation.1 | async-start | bytes 4718592 | tf_op jit(solution)/shard_map/all_gather | solution.py:62
  7.3 181.2 %all-gather.3.cloned.1.call-start = ((), (), s32[]{:S(2)}) async-start(), calls=%async_computation | async-start | bytes 4718592 | tf_op jit(solution)/shard_map/all_gather | solution.py:56
  8.0 31.4 %collective-permute-start.1 = (bf16[1024,256]{1,0:T(8,128)(2,1)}, bf16[1024,256]{1,0:T(8,128)(2,1)S(1)}, u32[]{:S(2)}, u32[]{:S(2)}) collective-permute-start(bf16[1024,256]{1,0:T(8,128)(2,1)} %param.11), channel_id=1, source_target_pairs={{0,1},{1,2},{2,3},{3,4},{4,5},{5,6},{6,7},{7,0},{8,9},{9,10},{10,1... | collective-permute-start | bytes 1572872 | tf_op jit(solution)/shard_map/ppermute | solution.py:21
  11.1 30.7 %collective-permute-start.5 = (bf16[1024,256]{1,0:T(8,128)(2,1)}, bf16[1024,256]{1,0:T(8,128)(2,1)S(1)}, u32[]{:S(2)}, u32[]{:S(2)}) collective-permute-start(bf16[1024,256]{1,0:T(8,128)(2,1)} %param.11), channel_id=1, source_target_pairs={{0,7},{1,0},{2,1},{3,2},{4,3},{5,4},{6,5},{7,6},{8,15},{9,8},{10,9... | collective-permute-start | bytes 1572872 | tf_op jit(solution)/shard_map/ppermute | solution.py:25
  39.4 2.4 %copy-start.4 = (bf16[1024,256]{1,0:T(8,128)(2,1)}, bf16[1024,256]{1,0:T(8,128)(2,1)S(1)}, u32[]{:S(2)}) copy-start(bf16[1024,256]{1,0:T(8,128)(2,1)S(1)} %collective-permute-done.1) | copy-start | bytes 1572868
  39.4 31.4 %collective-permute-start.2 = (bf16[1024,256]{1,0:T(8,128)(2,1)S(1)}, bf16[1024,256]{1,0:T(8,128)(2,1)S(1)}, u32[]{:S(2)}, u32[]{:S(2)}) collective-permute-start(bf16[1024,256]{1,0:T(8,128)(2,1)S(1)} %collective-permute-done.1), channel_id=1, source_target_pairs={{0,1},{1,2},{2,3},{3,4},{4,5},{5,6},{6,7},{7,0},{8,9},{9,10},{10,1... | collective-permute-start | bytes 1572872 | tf_op jit(solution)/shard_map/ppermute | solution.py:21
  41.8 78.2 %copy-start.2 = (bf16[1024,256]{1,0:T(8,128)(2,1)}, bf16[1024,256]{1,0:T(8,128)(2,1)S(1)}, u32[]{:S(2)}) copy-start(bf16[1024,256]{1,0:T(8,128)(2,1)S(1)} %collective-permute-done.5) | copy-start | bytes 1572868
  41.8 152.6 %collective-permute-start.6 = (bf16[1024,256]{1,0:T(8,128)(2,1)S(1)}, bf16[1024,256]{1,0:T(8,128)(2,1)}, u32[]{:S(2)}, u32[]{:S(2)}) collective-permute-start(bf16[1024,256]{1,0:T(8,128)(2,1)S(1)} %collective-permute-done.5), channel_id=1, source_target_pairs={{0,7},{1,0},{2,1},{3,2},{4,3},{5,4},{6,5},{7,6},{8,15},{9,8},{10,9... | collective-permute-start | bytes 1572872 | tf_op jit(solution)/shard_map/ppermute | solution.py:25
  70.8 49.1 %copy-start.6 = (bf16[1024,256]{1,0:T(8,128)(2,1)}, bf16[1024,256]{1,0:T(8,128)(2,1)S(1)}, u32[]{:S(2)}) copy-start(bf16[1024,256]{1,0:T(8,128)(2,1)S(1)} %collective-permute-done.2) | copy-start | bytes 1572868
  70.8 125.9 %collective-permute-start.3 = (bf16[1024,256]{1,0:T(8,128)(2,1)S(1)}, bf16[1024,256]{1,0:T(8,128)(2,1)}, u32[]{:S(2)}, u32[]{:S(2)}) collective-permute-start(bf16[1024,256]{1,0:T(8,128)(2,1)S(1)} %collective-permute-done.2), channel_id=1, source_target_pairs={{0,1},{1,2},{2,3},{3,4},{4,5},{5,6},{6,7},{7,0},{8,9},{9,10},{10,1... | collective-permute-start | bytes 1572872 | tf_op jit(solution)/shard_map/ppermute | solution.py:21
  119.9 74.4 %copy-start.8 = (bf16[1024]{0:T(1024)(128)(2,1)S(1)}, bf16[1024]{0:T(1024)(128)(2,1)}, u32[]{:S(2)}) copy-start(bf16[1024]{0:T(1024)(128)(2,1)} %param.10) | copy-start | bytes 6148
  193.1 3.7 %collective-permute-start = (bf16[1024,30]{0,1:T(8,128)(2,1)S(1)}, bf16[1024,30]{0,1:T(8,128)(2,1)S(1)}, u32[]{:S(2)}, u32[]{:S(2)}) collective-permute-start(bf16[1024,30]{0,1:T(8,128)(2,1)S(1)} %slice.6), channel_id=1, source_target_pairs={{0,8},{8,16},{16,24},{1,9},{9,17},{17,25},{2,10},{10,18},{18,26},{... | collective-permute-start | bytes 184328 | tf_op jit(solution)/shard_map/ppermute | solution.py:33
  194.4 32.2 %collective-permute-start.7 = (bf16[1024,256]{1,0:T(8,128)(2,1)}, bf16[1024,256]{1,0:T(8,128)(2,1)}, u32[]{:S(2)}, u32[]{:S(2)}) collective-permute-start(bf16[1024,256]{1,0:T(8,128)(2,1)} %collective-permute-done.6), channel_id=1, source_target_pairs={{0,7},{1,0},{2,1},{3,2},{4,3},{5,4},{6,5},{7,6},{8,15},{9,8},{10,9... | collective-permute-start | bytes 1572872 | tf_op jit(solution)/shard_map/ppermute | solution.py:25
  196.8 23.0 %collective-permute-start.4 = (bf16[1024,256]{1,0:T(8,128)(2,1)}, bf16[1024,256]{1,0:T(8,128)(2,1)}, u32[]{:S(2)}, u32[]{:S(2)}) collective-permute-start(bf16[1024,256]{1,0:T(8,128)(2,1)} %collective-permute-done.3), channel_id=1, source_target_pairs={{0,1},{1,2},{2,3},{3,4},{4,5},{5,6},{6,7},{7,0},{8,9},{9,10},{10,1... | collective-permute-start | bytes 1572872 | tf_op jit(solution)/shard_map/ppermute | solution.py:21
  197.0 0.8 copy-start.9
  197.1 0.8 copy-start.10
  206.1 16.9 %copy-start.7 = (bf16[1024,256]{1,0:T(8,128)(2,1)S(1)}, bf16[1024,256]{1,0:T(8,128)(2,1)}, u32[]{:S(2)}) copy-start(bf16[1024,256]{1,0:T(8,128)(2,1)} %copy-done.6) | copy-start | bytes 1572868
  206.6 16.8 %copy-start.5 = (bf16[1024,256]{1,0:T(8,128)(2,1)S(1)}, bf16[1024,256]{1,0:T(8,128)(2,1)}, u32[]{:S(2)}) copy-start(bf16[1024,256]{1,0:T(8,128)(2,1)} %copy-done.4) | copy-start | bytes 1572868
  221.3 2.7 %copy-start.1 = (bf16[1024,256]{1,0:T(8,128)(2,1)S(1)}, bf16[1024,256]{1,0:T(8,128)(2,1)}, u32[]{:S(2)}) copy-start(bf16[1024,256]{1,0:T(8,128)(2,1)} %param.11) | copy-start | bytes 1572868
  222.9 1.6 copy-start.3
Sparse Core Ops, SparseCore 0:
  9.5 105.3 all-gather.4
  116.9 71.5 all-gather.2
